TPU v7x, 32 devices: a whole 2x2x4 slice. The times are simulated.
32 devices in a mesh: sp: 8 (over z, y), tp: 4 (over x, core).
Axes of the slice: x: 2, y: 2, z: 4, core: 2. Of those that a mesh axis runs over, the one named last changes fastest.
Arguments:
- mixer_out: bfloat16 [1024, 2048], P('sp'), may hold values from -6 to 6
- conv_out: bfloat16 [1024, 2048], P('sp', 'tp'), may hold values from -350 to 350
- out_cot: bfloat16 [1024, 2048], P('sp'), may hold values from -6 to 6
- routes: int32 [1024, 2], P('sp'), may hold values from 0 to 7, all different within a row; in each aligned block of 128 rows (0 to 127, 128 to 255, ...) at most 64 rows name the same one
- route_weight: float32 [1024, 2], P('sp'), may hold values from 0.3 to 2.5
- gate_weight: bfloat16 [8, 2048, 1024], P('sp', None, 'tp'), may hold values from -0.125 to 0.125
- up_weight: bfloat16 [8, 2048, 1024], P('sp', None, 'tp'), may hold values from -0.125 to 0.125
- down_weight: bfloat16 [8, 1024, 2048], P('sp', 'tp'), may hold values from -0.1875 to 0.1875
- out_weight: bfloat16 [2048, 2048], P('tp'), may hold values from -0.125 to 0.125
- norm_gain: float32 [2048], P('tp'), may hold values from 0.1 to 1.9
- conv_taps: float32 [31, 2048], P(None, 'tp'), may hold values from -1 to 1
Outputs:
- gate_grad: bfloat16 [8, 2048, 1024], P('sp', None, 'tp')
- up_grad: bfloat16 [8, 2048, 1024], P('sp', None, 'tp')
- down_grad: bfloat16 [8, 1024, 2048], P('sp', 'tp')
- proj_grad: float32 [2048, 2048], P('sp', 'tp')
- gated_grad: float32 [1024, 2048], P('sp', 'tp')
Inputs may be any that keep to these rules, and one draw needn't show every extreme that they name: `routes`: each row names 2 different experts. Among the rows of one device no expert is named by more than 64 rows, and in every draw some expert is named by exactly 64 rows of some device.
All inputs are finite; a program needn't handle non-finite values.
Results may differ from a plain program's by a relative error of at most 0.0095.
Values may be sent and summed in bfloat16 or wider, within the bound.
A program may use at most 64 MiB of HBM per device.

v0:
```python
import jax
import jax.numpy as jnp
from jax import lax
from jax.sharding import PartitionSpec as P

norm_epsilon = 1e-05


def shifted(block, axis, distance):
    devices = range(lax.axis_size(axis))
    route = [(i - distance, i) for i in devices if i - distance in devices]
    return lax.ppermute(block, axis, route)


def expert_backward(x_rows, cot_rows, w_gate, w_up, w_down):
    pre_gate = jnp.dot(x_rows, w_gate, preferred_element_type=jnp.float32)
    pre_up = jnp.dot(x_rows, w_up, preferred_element_type=jnp.float32)
    sig_gate = jax.nn.sigmoid(pre_gate)
    activation = (pre_gate * sig_gate * pre_up).astype(jnp.bfloat16)
    down_g = lax.dot_general(
        activation, cot_rows, (((0,), (0,)), ((), ())), preferred_element_type=jnp.float32
    ).astype(jnp.bfloat16)
    act_grad = lax.dot_general(
        cot_rows, w_down, (((1,), (1,)), ((), ())), preferred_element_type=jnp.float32
    )
    gate_pre_grad = (act_grad * pre_up * sig_gate * (1.0 + pre_gate * (1.0 - sig_gate))).astype(
        jnp.bfloat16
    )
    up_pre_grad = (act_grad * pre_gate * sig_gate).astype(jnp.bfloat16)
    gate_g = lax.dot_general(
        x_rows, gate_pre_grad, (((0,), (0,)), ((), ())), preferred_element_type=jnp.float32
    ).astype(jnp.bfloat16)
    up_g = lax.dot_general(
        x_rows, up_pre_grad, (((0,), (0,)), ((), ())), preferred_element_type=jnp.float32
    ).astype(jnp.bfloat16)
    partial_value = lax.dot_general(
        gate_pre_grad, w_gate, (((1,), (1,)), ((), ())), preferred_element_type=jnp.float32
    )
    partial_value = partial_value + lax.dot_general(
        up_pre_grad, w_up, (((1,), (1,)), ((), ())), preferred_element_type=jnp.float32
    )
    rounded = lax.optimization_barrier(partial_value.astype(jnp.bfloat16))
    return (gate_g, up_g, down_g, rounded.astype(jnp.float32))


def on_device(
    mixer_out,
    conv_out,
    out_cot,
    routes,
    route_weight,
    gate_weight,
    up_weight,
    down_weight,
    out_weight,
    norm_gain,
    conv_taps,
):
    tokens_here, model_width = out_cot.shape
    route_count = routes.shape[1]
    experts = lax.axis_size("sp")
    capacity = 2 * tokens_here * route_count // experts
    quarter = conv_out.shape[1]
    first_col = lax.axis_index("tp") * quarter
    flat_routes = routes.reshape(-1)
    one_hot = (flat_routes[:, None] == jnp.arange(experts, dtype=jnp.int32)[None, :]).astype(
        jnp.int32
    )
    within = jnp.sum((jnp.cumsum(one_hot, axis=0) - one_hot) * one_hot, axis=1)
    slot_index = flat_routes * capacity + within
    row_cot = (route_weight[:, :, None] * out_cot[:, None, :].astype(jnp.float32)).astype(
        jnp.bfloat16
    )
    row_cot = row_cot.reshape(tokens_here * route_count, model_width)
    rows_input = jnp.repeat(mixer_out, route_count, axis=0)
    w_gate = gate_weight[0]
    w_up = up_weight[0]
    w_down = down_weight[0]
    rows_part = lax.dynamic_slice_in_dim(rows_input, first_col, quarter, 1)
    cot_part = lax.dynamic_slice_in_dim(row_cot, first_col, quarter, 1)
    send_rows = jnp.zeros((experts * capacity, quarter), jnp.bfloat16).at[slot_index].set(rows_part)
    send_cot = jnp.zeros((experts * capacity, quarter), jnp.bfloat16).at[slot_index].set(cot_part)
    rows_slice, cot_slice = (
        lax.all_to_all(send_rows, "sp", split_axis=0, concat_axis=0, tiled=True),
        lax.all_to_all(send_cot, "sp", split_axis=0, concat_axis=0, tiled=True),
    )
    x_rows, cot_rows = (
        lax.all_gather(rows_slice, "tp", axis=1, tiled=True),
        lax.all_gather(cot_slice, "tp", axis=1, tiled=True),
    )
    gate_g, up_g, down_g, partial_value = expert_backward(x_rows, cot_rows, w_gate, w_up, w_down)
    back_slice = lax.psum_scatter(
        partial_value.astype(jnp.bfloat16), "tp", scatter_dimension=1, tiled=True
    )
    returned = lax.all_to_all(back_slice, "sp", split_axis=0, concat_axis=0, tiled=True)
    picked = returned[slot_index].astype(jnp.float32).reshape(tokens_here, route_count, quarter)
    own_cot = lax.dynamic_slice_in_dim(out_cot, first_col, quarter, 1).astype(jnp.float32)
    mix_part = (own_cot + jnp.sum(picked, axis=1)).astype(jnp.bfloat16)
    mix_grad = lax.all_gather(mix_part, "tp", axis=1, tiled=True)
    conv_vals = conv_out.astype(jnp.float32)
    power_sum = lax.psum(jnp.sum(conv_vals * conv_vals, axis=1), "tp")
    inv_rms = lax.rsqrt(power_sum / model_width + norm_epsilon)[:, None]
    normed = conv_vals * inv_rms * norm_gain[None, :]
    sig_norm = jax.nn.sigmoid(normed)
    activated = (normed * sig_norm).astype(jnp.bfloat16)
    proj_grad = lax.psum_scatter(
        lax.dot_general(
            mix_grad, activated, (((0,), (0,)), ((), ())), preferred_element_type=jnp.float32
        ),
        "sp",
        scatter_dimension=0,
        tiled=True,
    )
    norm_in_grad = lax.dot_general(
        mix_grad, out_weight, (((1,), (1,)), ((), ())), preferred_element_type=jnp.float32
    )
    scaled = norm_in_grad * sig_norm * (1.0 + normed * (1.0 - sig_norm)) * norm_gain[None, :]
    dot_sum = lax.psum(jnp.sum(conv_vals * scaled, axis=1), "tp")
    conv_grad = inv_rms * scaled - conv_vals * inv_rms**3 * (dot_sum / model_width)[:, None]
    reach = conv_taps.shape[0] - 1
    following = shifted(conv_grad[:reach].astype(jnp.bfloat16), "sp", -1).astype(jnp.float32)
    extended = jnp.concatenate([conv_grad, following], axis=0)
    gated_grad = jnp.zeros((tokens_here, quarter), jnp.float32)
    for tap_index in range(reach + 1):
        gated_grad = (
            gated_grad
            + conv_taps[tap_index][None, :] * extended[tap_index : tap_index + tokens_here]
        )
    return (gate_g[None], up_g[None], down_g[None], proj_grad, gated_grad)


def solution(mesh):
    placed = (
        P("sp", None),
        P("sp", "tp"),
        P("sp", None),
        P("sp", None),
        P("sp", None),
        P("sp", None, "tp"),
        P("sp", None, "tp"),
        P("sp", "tp", None),
        P("tp", None),
        P("tp"),
        P(None, "tp"),
    )
    return jax.shard_map(
        on_device,
        mesh=mesh,
        in_specs=placed,
        out_specs=(
            P("sp", None, "tp"),
            P("sp", None, "tp"),
            P("sp", "tp", None),
            P("sp", "tp"),
            P("sp", "tp"),
        ),
        check_vma=False,
    )
```

profile of v0, /device:TPU:0, one launch (start us, length us, event | category | flops | bytes accessed | tf_op | source)
XLA Modules:
  0.0 249.0 jit_solution(12944334722822858562)
XLA Ops:
  7.2 0.8 broadcast_multiply_fusion
  8.0 0.8 copy.17
  8.8 0.1 eq.29
  9.0 0.1 eq.25
  9.1 0.1 copy.16
  9.2 0.1 mul.438
  9.4 0.6 reduce-window.6
  10.0 0.2 slice_reduce_fusion
  10.2 1.7 broadcast_in_dim.8
  11.9 1.2 reshape.83
  13.1 0.1 fusion.131
  13.2 2.1 scatter_custom_fusion
  15.3 21.7 %all_to_all.36 = bf16[8,64,512]{2,1,0:T(8,128)(2,1)} all-to-all(bf16[8,64,512]{2,1,0:T(8,128)(2,1)S(1)} %bitcast.85), channel_id=1, replica_groups=mesh['sp'=8,'tp'=4] {'sp'}, dimensions={0} | all-to-all | bytes 1048576 | tf_op jit(solution)/shard_map/all_to_all | solution.py:84
  37.1 2.4 mul.443
  39.5 3.7 %mul.444 = f32[256,2048]{1,0:T(8,128)} reshape(f32[128,2,2048]{2,1,0:T(2,128)} %mul.443) | data formatting | bytes 4194304 | tf_op jit(solution)/shard_map/mul | solution.py:71
  43.2 0.1 copy.19
  43.3 0.1 mul.441
  43.4 2.4 scatter_custom_fusion.1
  45.8 17.5 %all_to_all.37 = bf16[8,64,512]{2,1,0:T(8,128)(2,1)} all-to-all(bf16[8,64,512]{2,1,0:T(8,128)(2,1)S(1)} %bitcast.84), channel_id=1, replica_groups=mesh['sp'=8,'tp'=4] {'sp'}, dimensions={0} | all-to-all | bytes 1048576 | tf_op jit(solution)/shard_map/all_to_all | solution.py:85
  63.4 3.5 %fusion.7 = f32[512,256]{1,0:T(8,128)} fusion(bf16[512,2048]{1,0:T(8,128)(2,1)} %all-gather.3.cloned.1.call-done, bf16[1,2048,256]{2,1,0:T(8,128)(2,1)} %param.16), kind=kOutput, calls=%fused_computation.44 | convolution fusion | flops 536870912 | bytes 3670016 | tf_op jit(solution)/shard_map/dot_general | solution.py:16
  66.9 1.5 fusion.10
  68.4 16.7 %all-gather.5.cloned.1.call-done = bf16[512,2048]{1,0:T(8,128)(2,1)} async-done(((bf16[512,512]{1,0:T(8,128)(2,1)}), bf16[512,2048]{1,0:T(8,128)(2,1)}) %all-gather.5.cloned.1.call-update) | async-done | bytes 2097168 | tf_op jit(solution)/shard_map/all_gather | solution.py:89
  85.1 3.0 %multiply_convert_fusion.1 = (bf16[512,256]{1,0:T(8,128)(2,1)S(1)}, bf16[512,256]{1,0:T(8,128)(2,1)S(1)}) fusion(f32[512,256]{1,0:T(8,128)} %fusion.7, f32[512,256]{1,0:T(8,128)} %fusion.10, bf16[512,2048]{1,0:T(8,128)(2,1)} %all-gather.5.cloned.1.call-done, bf16[1,256,2048]{2,1,0:T(8,128)(2,1)} %param.18), kind=kOutput, calls=%fused_computation.83 | convolution fusion | flops 538574848 | bytes 4718592 | tf_op jit(solution)/shard_map/dot_general | solution.py:23
  88.1 0.7 fusion.5
  88.8 0.6 copy-done.5
  89.4 2.1 add_convert_fusion
  91.5 31.3 %reduce-scatter.3.cloned.1.call-done = bf16[512,512]{1,0:T(8,128)(2,1)} async-done(((bf16[512,2048]{1,0:T(8,128)(2,1)}), bf16[512,512]{1,0:T(8,128)(2,1)}) %reduce-scatter.3.cloned.1.call-update) | async-done | bytes 524304 | tf_op jit(solution)/shard_map/reduce_scatter | solution.py:92
  122.8 5.5 %all-to-all-start.2 = ((bf16[8,64,512]{2,1,0:T(8,128)(2,1)}), bf16[8,64,512]{2,1,0:T(8,128)(2,1)S(1)}, u32[]{:S(2)}, u32[]{:S(2)}) async-start(bf16[8,64,512]{2,1,0:T(8,128)(2,1)} %bitcast.86), calls=%async_computation.3 | async-start | bytes 1048576 | tf_op jit(solution)/shard_map/all_to_all | solution.py:95
  128.4 0.1 fusion.15
  128.5 6.0 %psum.14 = f32[128]{0:T(128)S(1)} all-reduce(f32[128]{0:T(128)S(1)} %fusion.15), channel_id=1, replica_groups=mesh['sp'=8,'tp'=4] {'tp'}, use_global_device_ids=true, to_apply=%region_8.9 | all-reduce | flops 128 | bytes 1024 | tf_op jit(solution)/shard_map/psum | solution.py:101
  134.5 8.2 %all-to-all-done.2 = bf16[8,64,512]{2,1,0:T(8,128)(2,1)S(1)} async-done(((bf16[8,64,512]{2,1,0:T(8,128)(2,1)}), bf16[8,64,512]{2,1,0:T(8,128)(2,1)S(1)}, u32[]{:S(2)}, u32[]{:S(2)}) %all-to-all-start.2) | async-done | bytes 524320 | tf_op jit(solution)/shard_map/all_to_all | solution.py:95
  142.7 1.2 gather_fusion
  143.8 0.3 reshape.84
  144.2 0.6 reduce_sum.40
  144.8 0.9 add_convert_fusion.1
  145.7 6.7 %all_gather.11 = bf16[128,2048]{1,0:T(8,128)(2,1)S(1)} all-gather(bf16[128,512]{1,0:T(8,128)(2,1)S(1)} %add_convert_fusion.1), channel_id=1, replica_groups=mesh['sp'=8,'tp'=4] {'tp'}, dimensions={1}, use_global_device_ids=true | all-gather | bytes 655360 | tf_op jit(solution)/shard_map/all_gather | solution.py:99
  152.4 2.8 %fusion.125 = f32[2048,512]{1,0:T(8,128)} fusion(bf16[128,2048]{1,0:T(8,128)(2,1)S(1)} %all_gather.11, bf16[128,512]{1,0:T(8,128)(2,1)S(1)} %copy-done.2, f32[512]{0:T(512)S(1)} %copy-done.12, f32[128]{0:T(128)S(1)} %get-tuple-element.39), kind=kOutput, calls=%fused_computation.201 | convolution fusion | flops 268959744 | bytes 4852224 | tf_op jit(solution)/shard_map/dot_general | solution.py:107
  155.2 0.8 copy-done.11
  156.2 3.5 %fusion = bf16[1,2048,256]{2,1,0:T(8,128)(2,1)} fusion(bf16[512,2048]{1,0:T(8,128)(2,1)} %all-gather.3.cloned.1.call-done, bf16[512,256]{1,0:T(8,128)(2,1)S(1)} %get-tuple-element.6), kind=kOutput, calls=%fused_computation.36 | convolution fusion | flops 537395200 | bytes 3407872 | tf_op jit(solution)/shard_map/dot_general | solution.py:30
  159.6 1.8 fusion.2
  161.4 0.9 fusion.27
  162.3 7.2 %psum.15 = f32[128]{0:T(128)S(1)} all-reduce(f32[128]{0:T(128)S(1)} %get-tuple-element.40), channel_id=1, replica_groups=mesh['sp'=8,'tp'=4] {'tp'}, use_global_device_ids=true, to_apply=%region_11.12 | all-reduce | flops 128 | bytes 1024 | tf_op jit(solution)/shard_map/psum | solution.py:118
  169.6 0.1 fusion.26
  169.7 1.3 collective-permute-start
  171.0 3.3 %fusion.1 = bf16[1,2048,256]{2,1,0:T(8,128)(2,1)} fusion(bf16[512,2048]{1,0:T(8,128)(2,1)} %all-gather.3.cloned.1.call-done, bf16[512,256]{1,0:T(8,128)(2,1)S(1)} %copy-done.10), kind=kOutput, calls=%fused_computation.37 | convolution fusion | flops 537395200 | bytes 3407872 | tf_op jit(solution)/shard_map/dot_general | solution.py:33
  174.4 1.1 collective-permute-done
  175.5 1.4 fusion.33
  176.9 65.6 %reduce-scatter.5.cloned.1.call-done = f32[256,512]{1,0:T(8,128)} async-done(((f32[2048,512]{1,0:T(8,128)}), f32[256,512]{1,0:T(8,128)}) %reduce-scatter.5.cloned.1.call-update) | async-done | bytes 524304 | tf_op jit(solution)/shard_map/reduce_scatter | solution.py:106
  (48 shorter events, 0.4 us)
Async XLA Ops:
  7.2 154.2 %copy-start = (bf16[512,2048]{1,0:T(8,128)(2,1)S(1)}, bf16[512,2048]{1,0:T(8,128)(2,1)}, u32[]{:S(2)}) copy-start(bf16[512,2048]{1,0:T(8,128)(2,1)} %param.19) | copy-start | bytes 6291460
  7.2 56.2 %all-gather.3.cloned.1.call-start = ((), (), s32[]{:S(2)}) async-start(), calls=%async_computation.5 | async-start | bytes 2621440 | tf_op jit(solution)/shard_map/all_gather | solution.py:88
  13.1 24.0 %copy-start.6 = (bf16[128,2048]{1,0:T(8,128)(2,1)S(1)}, bf16[128,2048]{1,0:T(8,128)(2,1)}, u32[]{:S(2)}) copy-start(bf16[128,2048]{1,0:T(8,128)(2,1)} %param.13) | copy-start | bytes 1572868
  37.1 48.0 %all-gather.5.cloned.1.call-start = ((), (), s32[]{:S(2)}) async-start(), calls=%async_computation.6 | async-start | bytes 2621440 | tf_op jit(solution)/shard_map/all_gather | solution.py:89
  39.5 3.7 %copy-start.13 = (f32[128,2]{0,1:T(2,128)S(1)}, f32[128,2]{0,1:T(2,128)}, u32[]{:S(2)}) copy-start(f32[128,2]{0,1:T(2,128)} %param.15) | copy-start | bytes 3076
  63.3 3.6 %copy-start.4 = (bf16[1,2048,256]{2,1,0:T(8,128)(2,1)S(1)}, bf16[1,2048,256]{2,1,0:T(8,128)(2,1)}, u32[]{:S(2)}) copy-start(bf16[1,2048,256]{2,1,0:T(8,128)(2,1)} %param.17) | copy-start | bytes 3145732
  63.3 59.5 %reduce-scatter.3.cloned.1.call-start = ((), (), s32[]{:S(2)}) async-start(), calls=%async_computation.7 | async-start | bytes 2621440 | tf_op jit(solution)/shard_map/reduce_scatter | solution.py:92
  63.4 3.5 %copy-start.14 = (bf16[512,2048]{1,0:T(8,128)(2,1)S(1)}, bf16[512,2048]{1,0:T(8,128)(2,1)}, u32[]{:S(2)}) copy-start(bf16[512,2048]{1,0:T(8,128)(2,1)} %all-gather.3.cloned.1.call-done) | copy-start | bytes 6291460
  68.4 19.6 %copy-start.3 = (bf16[1,2048,256]{2,1,0:T(8,128)(2,1)S(1)}, bf16[1,2048,256]{2,1,0:T(8,128)(2,1)}, u32[]{:S(2)}) copy-start(bf16[1,2048,256]{2,1,0:T(8,128)(2,1)} %param.16) | copy-start | bytes 3145732
  88.1 0.8 copy-start.9
  88.1 1.3 copy-start.5
  91.5 36.9 %copy-start.2 = (bf16[128,512]{1,0:T(8,128)(2,1)S(1)}, bf16[128,512]{1,0:T(8,128)(2,1)}, u32[]{:S(2)}) copy-start(bf16[128,512]{1,0:T(8,128)(2,1)} %param.12) | copy-start | bytes 393220
  122.8 19.8 %all-to-all-start.2 = ((bf16[8,64,512]{2,1,0:T(8,128)(2,1)}), bf16[8,64,512]{2,1,0:T(8,128)(2,1)S(1)}, u32[]{:S(2)}, u32[]{:S(2)}) async-start(bf16[8,64,512]{2,1,0:T(8,128)(2,1)} %bitcast.86), calls=%async_computation.3 | async-start | bytes 1048576 | tf_op jit(solution)/shard_map/all_to_all | solution.py:95
  128.4 114.1 %reduce-scatter.5.cloned.1.call-start = ((), (), s32[]{:S(2)}) async-start(), calls=%async_computation.8 | async-start | bytes 4718592 | tf_op jit(solution)/shard_map/reduce_scatter | solution.py:106
  142.7 9.7 %copy-start.12 = (f32[512]{0:T(512)S(1)}, f32[512]{0:T(512)}, u32[]{:S(2)}) copy-start(f32[512]{0:T(512)} %param.20) | copy-start | bytes 6148
  155.2 0.8 copy-start.11
  156.1 3.5 %copy-start.1 = (bf16[512,2048]{1,0:T(8,128)(2,1)S(1)}, bf16[512,2048]{1,0:T(8,128)(2,1)}, u32[]{:S(2)}) copy-start(bf16[512,2048]{1,0:T(8,128)(2,1)} %all-gather.5.cloned.1.call-done) | copy-start | bytes 6291460
  156.1 3.5 %copy-start.7 = (f32[512,256]{1,0:T(8,128)S(1)}, f32[512,256]{1,0:T(8,128)}, u32[]{:S(2)}) copy-start(f32[512,256]{1,0:T(8,128)} %fusion.7) | copy-start | bytes 1572868
  156.1 3.5 %copy-start.8 = (f32[512,256]{1,0:T(8,128)S(1)}, f32[512,256]{1,0:T(8,128)}, u32[]{:S(2)}) copy-start(f32[512,256]{1,0:T(8,128)} %fusion.10) | copy-start | bytes 1572868
  161.4 9.6 %copy-start.10 = (bf16[512,256]{1,0:T(8,128)(2,1)S(1)}, bf16[512,256]{1,0:T(8,128)(2,1)}, u32[]{:S(2)}) copy-start(bf16[512,256]{1,0:T(8,128)(2,1)} %copy-done.9) | copy-start | bytes 786436
  169.7 5.8 %collective-permute-start = (bf16[30,512]{1,0:T(8,128)(2,1)S(1)}, bf16[30,512]{1,0:T(8,128)(2,1)S(1)}, u32[]{:S(2)}, u32[]{:S(2)}) collective-permute-start(bf16[30,512]{1,0:T(8,128)(2,1)S(1)} %slice.713), channel_id=1, source_target_pairs={{4,0},{8,4},{12,8},{16,12},{20,16},{24,20},{28,24},{5,1},{9,5},{13... | collective-permute-start | bytes 92168 | tf_op jit(solution)/shard_map/ppermute | solution.py:12
Sparse Core Ops, SparseCore 0:
  37.2 21.5 all-gather.2
  63.5 21.6 all-gather.4
  91.6 31.1 reduce-scatter.2
  155.4 87.0 reduce-scatter.4
where the time goes:
time: 250 us; the launch traced here: 249 us
  waiting for transfers between devices  123 us (49%)
  blocking collectives  59.1 us (24%)
  matrix products  23.1 us (9%)
  local copies, waits for them, and re-layouts  15.8 us (6%)
  between operations  14 us (6%)
  other arithmetic  7.12 us (3%)
  starting transfers between devices  6.97 us (3%)
    reduce_scatter x1, waiting for transfers between devices, on_device(): lax.psum_scatter(lax.dot_general(mix_grad, activated, (((0,), (0,)), ((),...  65.6 us
    reduce_scatter x1, waiting for transfers between devices, on_device(): lax.psum_scatter(partial_value.astype(jnp.bfloat16), 'tp', scatter_dimens...  31.3 us
    all_to_all x1, blocking collectives, on_device(): lax.all_to_all(send_rows, 'sp', split_axis=0, concat_axis=0, tiled=True)  21.7 us
    all_to_all x1, blocking collectives, on_device(): lax.all_to_all(send_cot, 'sp', split_axis=0, concat_axis=0, tiled=True)  17.5 us
    all_gather x1, waiting for transfers between devices, on_device(): lax.all_gather(cot_slice, 'tp', axis=1, tiled=True)  16.7 us
    all_to_all x1, waiting for transfers between devices, on_device(): lax.all_to_all(back_slice, 'sp', split_axis=0, concat_axis=0, tiled=True)  8.16 us
    psum x1, blocking collectives, on_device(): dot_sum = lax.psum(jnp.sum(conv_vals * scaled, axis=1), 'tp')  7.21 us
    all_gather x1, blocking collectives, on_device(): mix_grad = lax.all_gather(mix_part, 'tp', axis=1, tiled=True)  6.68 us
  transfers between devices with their start and end apart: 6, of which 5 were waited for; matrix products, arithmetic and copies ran while one was open for 10% of the time, Pallas kernels for 0%

commit v1 on v0

--- a/solution.py
+++ b/solution.py
@@ -86,7 +86,7 @@
     )
     x_rows, cot_rows = (
         lax.all_gather(rows_slice, "tp", axis=1, tiled=True),
-        lax.all_gather(cot_slice, "tp", axis=1, tiled=True),
+        jnp.concatenate(lax.all_gather(cot_slice, "tp"), axis=1),
     )
     gate_g, up_g, down_g, partial_value = expert_backward(x_rows, cot_rows, w_gate, w_up, w_down)
     back_slice = lax.psum_scatter(

time: 250 us -> 253 us (1.012)
  local copies, waits for them, and re-layouts: 15.8 us -> 19.4 us
    all_gather x0 -> x1, local copies, waits for them, and re-layouts: none -> 4.16 us  [on_device(): lax.all_gather(cot_slice, 'tp')]
where the time goes in v1:
time: 253 us
  waiting for transfers between devices  123 us (49%)
  blocking collectives  59.1 us (23%)
  matrix products  23.2 us (9%)
  local copies, waits for them, and re-layouts  19.4 us (8%)
  between operations  14 us (6%)
  other arithmetic  7.13 us (3%)
  starting transfers between devices  6.97 us (3%)
    reduce_scatter x1, waiting for transfers between devices, on_device(): lax.psum_scatter(lax.dot_general(mix_grad, activated, (((0,), (0,)), ((),...  65.6 us
    reduce_scatter x1, waiting for transfers between devices, on_device(): lax.psum_scatter(partial_value.astype(jnp.bfloat16), 'tp', scatter_dimens...  31.3 us
    all_to_all x1, blocking collectives, on_device(): lax.all_to_all(send_rows, 'sp', split_axis=0, concat_axis=0, tiled=True)  21.7 us
    all_to_all x1, blocking collectives, on_device(): lax.all_to_all(send_cot, 'sp', split_axis=0, concat_axis=0, tiled=True)  17.5 us
    all_gather x1, waiting for transfers between devices, on_device(): lax.all_gather(cot_slice, 'tp')  16.7 us
    all_to_all x1, waiting for transfers between devices, on_device(): lax.all_to_all(back_slice, 'sp', split_axis=0, concat_axis=0, tiled=True)  8.17 us
    psum x1, blocking collectives, on_device(): dot_sum = lax.psum(jnp.sum(conv_vals * scaled, axis=1), 'tp')  7.21 us
    all_gather x1, blocking collectives, on_device(): mix_grad = lax.all_gather(mix_part, 'tp', axis=1, tiled=True)  6.68 us
  transfers between devices with their start and end apart: 6, of which 5 were waited for; matrix products, arithmetic and copies ran while one was open for 10% of the time, Pallas kernels for 0%

profile of v1, /device:TPU:0, one launch (start us, length us, event | category | flops | bytes accessed | tf_op | source)
XLA Modules:
  0.0 252.7 jit_solution(11812643183610007828)
XLA Ops:
  7.2 0.8 broadcast_multiply_fusion
  8.0 0.8 copy.28
  8.8 0.1 eq.29
  9.0 0.1 eq.25
  9.1 0.1 copy.27
  9.2 0.1 mul.438
  9.4 0.6 reduce-window.6
  10.0 0.2 slice_reduce_fusion
  10.2 1.7 broadcast_in_dim.8
  11.9 1.2 reshape.90
  13.1 0.1 fusion.131
  13.2 2.1 scatter_custom_fusion
  15.3 21.7 %all_to_all.33 = bf16[8,64,512]{2,1,0:T(8,128)(2,1)} all-to-all(bf16[8,64,512]{2,1,0:T(8,128)(2,1)S(1)} %bitcast.90), channel_id=1, replica_groups=mesh['sp'=8,'tp'=4] {'sp'}, dimensions={0} | all-to-all | bytes 1048576 | tf_op jit(solution)/shard_map/all_to_all | solution.py:84
  37.1 2.4 mul.443
  39.6 3.7 %mul.444 = f32[256,2048]{1,0:T(8,128)} reshape(f32[128,2,2048]{2,1,0:T(2,128)} %mul.443) | data formatting | bytes 4194304 | tf_op jit(solution)/shard_map/mul | solution.py:71
  43.2 0.1 copy.30
  43.3 0.1 mul.441
  43.5 2.4 scatter_custom_fusion.1
  45.9 17.5 %all_to_all.34 = bf16[8,64,512]{2,1,0:T(8,128)(2,1)} all-to-all(bf16[8,64,512]{2,1,0:T(8,128)(2,1)S(1)} %bitcast.89), channel_id=1, replica_groups=mesh['sp'=8,'tp'=4] {'sp'}, dimensions={0} | all-to-all | bytes 1048576 | tf_op jit(solution)/shard_map/all_to_all | solution.py:85
  63.5 3.5 %fusion.7 = f32[512,256]{1,0:T(8,128)} fusion(bf16[512,2048]{1,0:T(8,128)(2,1)} %all-gather.3.cloned.1.call-done, bf16[1,2048,256]{2,1,0:T(8,128)(2,1)} %param.16), kind=kOutput, calls=%fused_computation.44 | convolution fusion | flops 536870912 | bytes 3670016 | tf_op jit(solution)/shard_map/dot_general | solution.py:16
  67.0 1.5 fusion.10
  68.5 16.7 %all-gather.5.cloned.1.call-done = bf16[4,512,512]{2,1,0:T(8,128)(2,1)} async-done(((bf16[1,512,512]{2,1,0:T(8,128)(2,1)}), bf16[4,512,512]{2,1,0:T(8,128)(2,1)}) %all-gather.5.cloned.1.call-update) | async-done | bytes 2097168 | tf_op jit(solution)/shard_map/all_gather | solution.py:89
  85.1 4.2 %copy.31 = bf16[4,512,512]{1,2,0:T(8,128)(2,1)} copy(bf16[4,512,512]{2,1,0:T(8,128)(2,1)} %all-gather.5.cloned.1.call-done) | data formatting | bytes 4194304 | tf_op jit(solution)/shard_map/all_gather | solution.py:89
  89.3 3.0 %multiply_convert_fusion.1 = (bf16[512,256]{1,0:T(8,128)(2,1)S(1)}, bf16[512,256]{1,0:T(8,128)(2,1)S(1)}) fusion(f32[512,256]{1,0:T(8,128)} %fusion.7, f32[512,256]{1,0:T(8,128)} %fusion.10, bf16[512,2048]{0,1:T(8,128)(2,1)} %bitcast.85, bf16[1,256,2048]{2,1,0:T(8,128)(2,1)} %param.18), kind=kOutput, calls=%fused_computation.83 | convolution fusion | flops 538574848 | bytes 4718592 | tf_op jit(solution)/shard_map/dot_general | solution.py:23
  92.4 0.7 fusion.5
  93.1 2.1 add_convert_fusion
  95.3 31.3 %reduce-scatter.3.cloned.1.call-done = bf16[512,512]{1,0:T(8,128)(2,1)} async-done(((bf16[512,2048]{1,0:T(8,128)(2,1)}), bf16[512,512]{1,0:T(8,128)(2,1)}) %reduce-scatter.3.cloned.1.call-update) | async-done | bytes 524304 | tf_op jit(solution)/shard_map/reduce_scatter | solution.py:92
  126.6 5.5 %all-to-all-start.2 = ((bf16[8,64,512]{2,1,0:T(8,128)(2,1)}), bf16[8,64,512]{2,1,0:T(8,128)(2,1)S(1)}, u32[]{:S(2)}, u32[]{:S(2)}) async-start(bf16[8,64,512]{2,1,0:T(8,128)(2,1)} %bitcast.91), calls=%async_computation.3 | async-start | bytes 1048576 | tf_op jit(solution)/shard_map/all_to_all | solution.py:95
  132.2 0.1 fusion.15
  132.3 6.0 %psum.14 = f32[128]{0:T(128)S(1)} all-reduce(f32[128]{0:T(128)S(1)} %fusion.15), channel_id=1, replica_groups=mesh['sp'=8,'tp'=4] {'tp'}, use_global_device_ids=true, to_apply=%region_8.9 | all-reduce | flops 128 | bytes 1024 | tf_op jit(solution)/shard_map/psum | solution.py:101
  138.3 8.2 %all-to-all-done.2 = bf16[8,64,512]{2,1,0:T(8,128)(2,1)S(1)} async-done(((bf16[8,64,512]{2,1,0:T(8,128)(2,1)}), bf16[8,64,512]{2,1,0:T(8,128)(2,1)S(1)}, u32[]{:S(2)}, u32[]{:S(2)}) %all-to-all-start.2) | async-done | bytes 524320 | tf_op jit(solution)/shard_map/all_to_all | solution.py:95
  146.4 1.2 gather_fusion
  147.6 0.3 reshape.93
  147.9 0.6 reduce_sum.40
  148.6 0.9 add_convert_fusion.1
  149.5 6.7 %all_gather.15 = bf16[128,2048]{1,0:T(8,128)(2,1)S(1)} all-gather(bf16[128,512]{1,0:T(8,128)(2,1)S(1)} %add_convert_fusion.1), channel_id=1, replica_groups=mesh['sp'=8,'tp'=4] {'tp'}, dimensions={1}, use_global_device_ids=true | all-gather | bytes 655360 | tf_op jit(solution)/shard_map/all_gather | solution.py:99
  156.2 2.8 %fusion.125 = f32[2048,512]{1,0:T(8,128)} fusion(bf16[128,2048]{1,0:T(8,128)(2,1)S(1)} %all_gather.15, bf16[128,512]{1,0:T(8,128)(2,1)S(1)} %copy-done.2, f32[512]{0:T(512)S(1)} %copy-done.9, f32[128]{0:T(128)S(1)} %get-tuple-element.39), kind=kOutput, calls=%fused_computation.201 | convolution fusion | flops 268959744 | bytes 4852224 | tf_op jit(solution)/shard_map/dot_general | solution.py:107
  159.0 0.8 copy-done.8
  159.9 3.5 %fusion = bf16[1,2048,256]{2,1,0:T(8,128)(2,1)} fusion(bf16[512,2048]{1,0:T(8,128)(2,1)} %all-gather.3.cloned.1.call-done, bf16[512,256]{1,0:T(8,128)(2,1)S(1)} %get-tuple-element.6), kind=kOutput, calls=%fused_computation.36 | convolution fusion | flops 537395200 | bytes 3407872 | tf_op jit(solution)/shard_map/dot_general | solution.py:30
  163.4 1.7 fusion.2
  165.1 0.9 fusion.27
  166.1 7.2 %psum.15 = f32[128]{0:T(128)S(1)} all-reduce(f32[128]{0:T(128)S(1)} %get-tuple-element.40), channel_id=1, replica_groups=mesh['sp'=8,'tp'=4] {'tp'}, use_global_device_ids=true, to_apply=%region_11.12 | all-reduce | flops 128 | bytes 1024 | tf_op jit(solution)/shard_map/psum | solution.py:118
  173.3 0.1 fusion.26
  173.4 1.3 collective-permute-start
  174.7 3.3 %fusion.1 = bf16[1,2048,256]{2,1,0:T(8,128)(2,1)} fusion(bf16[512,2048]{1,0:T(8,128)(2,1)} %all-gather.3.cloned.1.call-done, bf16[512,256]{1,0:T(8,128)(2,1)S(1)} %copy-done.7), kind=kOutput, calls=%fused_computation.37 | convolution fusion | flops 537395200 | bytes 3407872 | tf_op jit(solution)/shard_map/dot_general | solution.py:33
  178.1 1.2 collective-permute-done
  179.2 1.4 fusion.33
  180.6 65.6 %reduce-scatter.5.cloned.1.call-done = f32[256,512]{1,0:T(8,128)} async-done(((f32[2048,512]{1,0:T(8,128)}), f32[256,512]{1,0:T(8,128)}) %reduce-scatter.5.cloned.1.call-update) | async-done | bytes 524304 | tf_op jit(solution)/shard_map/reduce_scatter | solution.py:106
  (47 shorter events, 0.4 us)
Async XLA Ops:
  7.2 158.0 %copy-start = (bf16[512,2048]{1,0:T(8,128)(2,1)S(1)}, bf16[512,2048]{1,0:T(8,128)(2,1)}, u32[]{:S(2)}) copy-start(bf16[512,2048]{1,0:T(8,128)(2,1)} %param.19) | copy-start | bytes 6291460
  7.2 56.3 %all-gather.3.cloned.1.call-start = ((), (), s32[]{:S(2)}) async-start(), calls=%async_computation.5 | async-start | bytes 2621440 | tf_op jit(solution)/shard_map/all_gather | solution.py:88
  13.1 24.0 %copy-start.5 = (bf16[128,2048]{1,0:T(8,128)(2,1)S(1)}, bf16[128,2048]{1,0:T(8,128)(2,1)}, u32[]{:S(2)}) copy-start(bf16[128,2048]{1,0:T(8,128)(2,1)} %param.13) | copy-start | bytes 1572868
  37.1 48.1 %all-gather.5.cloned.1.call-start = ((), (), s32[]{:S(2)}) async-start(), calls=%async_computation.6 | async-start | bytes 2621440 | tf_op jit(solution)/shard_map/all_gather | solution.py:89
  39.6 3.7 %copy-start.10 = (f32[128,2]{0,1:T(2,128)S(1)}, f32[128,2]{0,1:T(2,128)}, u32[]{:S(2)}) copy-start(f32[128,2]{0,1:T(2,128)} %param.15) | copy-start | bytes 3076
  63.4 3.6 %copy-start.4 = (bf16[1,2048,256]{2,1,0:T(8,128)(2,1)S(1)}, bf16[1,2048,256]{2,1,0:T(8,128)(2,1)}, u32[]{:S(2)}) copy-start(bf16[1,2048,256]{2,1,0:T(8,128)(2,1)} %param.17) | copy-start | bytes 3145732
  63.4 63.2 %reduce-scatter.3.cloned.1.call-start = ((), (), s32[]{:S(2)}) async-start(), calls=%async_computation.7 | async-start | bytes 2621440 | tf_op jit(solution)/shard_map/reduce_scatter | solution.py:92
  63.5 3.5 %copy-start.11 = (bf16[512,2048]{1,0:T(8,128)(2,1)S(1)}, bf16[512,2048]{1,0:T(8,128)(2,1)}, u32[]{:S(2)}) copy-start(bf16[512,2048]{1,0:T(8,128)(2,1)} %all-gather.3.cloned.1.call-done) | copy-start | bytes 6291460
  89.3 3.1 %copy-start.3 = (bf16[1,2048,256]{2,1,0:T(8,128)(2,1)S(1)}, bf16[1,2048,256]{2,1,0:T(8,128)(2,1)}, u32[]{:S(2)}) copy-start(bf16[1,2048,256]{2,1,0:T(8,128)(2,1)} %param.16) | copy-start | bytes 3145732
  92.4 0.8 copy-start.6
  95.2 36.9 %copy-start.2 = (bf16[128,512]{1,0:T(8,128)(2,1)S(1)}, bf16[128,512]{1,0:T(8,128)(2,1)}, u32[]{:S(2)}) copy-start(bf16[128,512]{1,0:T(8,128)(2,1)} %param.12) | copy-start | bytes 393220
  126.6 19.8 %all-to-all-start.2 = ((bf16[8,64,512]{2,1,0:T(8,128)(2,1)}), bf16[8,64,512]{2,1,0:T(8,128)(2,1)S(1)}, u32[]{:S(2)}, u32[]{:S(2)}) async-start(bf16[8,64,512]{2,1,0:T(8,128)(2,1)} %bitcast.91), calls=%async_computation.3 | async-start | bytes 1048576 | tf_op jit(solution)/shard_map/all_to_all | solution.py:95
  132.1 114.1 %reduce-scatter.5.cloned.1.call-start = ((), (), s32[]{:S(2)}) async-start(), calls=%async_computation.8 | async-start | bytes 4718592 | tf_op jit(solution)/shard_map/reduce_scatter | solution.py:106
  146.4 9.7 %copy-start.9 = (f32[512]{0:T(512)S(1)}, f32[512]{0:T(512)}, u32[]{:S(2)}) copy-start(f32[512]{0:T(512)} %param.20) | copy-start | bytes 6148
  158.9 0.8 copy-start.8
  159.8 3.5 %copy-start.1 = (bf16[4,512,512]{1,2,0:T(8,128)(2,1)S(1)}, bf16[4,512,512]{1,2,0:T(8,128)(2,1)}, u32[]{:S(2)}) copy-start(bf16[4,512,512]{1,2,0:T(8,128)(2,1)} %copy.31) | copy-start | bytes 6291460
  159.9 3.5 %copy-start.12 = (f32[512,256]{1,0:T(8,128)S(1)}, f32[512,256]{1,0:T(8,128)}, u32[]{:S(2)}) copy-start(f32[512,256]{1,0:T(8,128)} %fusion.7) | copy-start | bytes 1572868
  159.9 3.5 %copy-start.13 = (f32[512,256]{1,0:T(8,128)S(1)}, f32[512,256]{1,0:T(8,128)}, u32[]{:S(2)}) copy-start(f32[512,256]{1,0:T(8,128)} %fusion.10) | copy-start | bytes 1572868
  165.1 9.6 %copy-start.7 = (bf16[512,256]{1,0:T(8,128)(2,1)S(1)}, bf16[512,256]{1,0:T(8,128)(2,1)}, u32[]{:S(2)}) copy-start(bf16[512,256]{1,0:T(8,128)(2,1)} %copy-done.6) | copy-start | bytes 786436
  173.4 5.8 %collective-permute-start = (bf16[30,512]{1,0:T(8,128)(2,1)S(1)}, bf16[30,512]{1,0:T(8,128)(2,1)S(1)}, u32[]{:S(2)}, u32[]{:S(2)}) collective-permute-start(bf16[30,512]{1,0:T(8,128)(2,1)S(1)} %slice.713), channel_id=1, source_target_pairs={{4,0},{8,4},{12,8},{16,12},{20,16},{24,20},{28,24},{5,1},{9,5},{13... | collective-permute-start | bytes 92168 | tf_op jit(solution)/shard_map/ppermute | solution.py:12
Sparse Core Ops, SparseCore 0:
  37.2 21.5 all-gather.2
  63.5 21.5 all-gather.4
  95.4 31.1 reduce-scatter.2
  159.1 87.0 reduce-scatter.4
